TPU v7x, 512 devices: a whole 4x8x8 slice. The times are simulated.
512 devices in a mesh: ep: 128 (over z, y, core), tp: 4 (over x).
Axes of the slice: x: 4, y: 8, z: 8, core: 2. Of those that a mesh axis runs over, the one named last changes fastest.
Arguments:
- resid: bfloat16 [2048, 2048], P('ep'), may hold values from -40 to 40
- queries: bfloat16 [2048, 1024], P('ep', 'tp'), may hold values from -146 to 146
- new_keys: bfloat16 [2048, 512], P('ep', 'tp'), may hold values from -6 to 6
- new_values: bfloat16 [2048, 512], P('ep', 'tp'), may hold values from -18 to 18
- key_cache: bfloat16 [2048, 4, 256, 128], P('ep', 'tp'), may hold values from -5 to 5
- value_cache: bfloat16 [2048, 4, 256, 128], P('ep', 'tp'), may hold values from -18 to 18
- cum_gate: float32 [2048, 8, 256], P('ep', 'tp'), may hold values from -256 to 0, as said below
- forget_logit: float32 [2048, 8], P('ep', 'tp'), may hold values from -6 to 6
- forget_bias: float32 [8], P('tp'), may hold values from -3 to 2
- lengths: int32 [2048], P('ep'), may hold values from 32 to 256
- out_weight: bfloat16 [1024, 2048], P('tp'), may hold values from -0.1875 to 0.1875
- norm_gain: float32 [2048], replicated, may hold values from 0.1 to 1.9
- mix_vector: bfloat16 [2048], replicated, may hold values from -0.125 to 0.125
- routes: int32 [2048, 2], P('ep'), may hold values from 0 to 31, all different within a row; in each aligned block of 16 rows (0 to 15, 16 to 31, ...) at most 2 rows name the same one
- route_weight: float32 [2048, 2], P('ep'), may hold values from 0.2 to 1
- expert_gate: bfloat16 [128, 2048, 768], P('ep', 'tp'), may hold values from -0.125 to 0.125
- expert_up: bfloat16 [128, 2048, 768], P('ep', 'tp'), may hold values from -0.125 to 0.125
- expert_down: bfloat16 [128, 768, 2048], P('ep', None, 'tp'), may hold values from -0.109375 to 0.109375
- dense_gate: bfloat16 [2048, 3072], P('tp', 'ep'), may hold values from -0.125 to 0.125
- dense_up: bfloat16 [2048, 3072], P('tp', 'ep'), may hold values from -0.125 to 0.125
- dense_down: bfloat16 [3072, 2048], P('ep', 'tp'), may hold values from -0.109375 to 0.109375
Outputs:
- layer_out: bfloat16 [2048, 2048], P('ep', 'tp')
Inputs may be any that keep to these rules, and one draw needn't show every extreme that they name: `routes`: each row names 2 different experts; the rows of one index of ep name no expert more than 2 times. `cum_gate`: for positions below the sequence's length, the running sum of the log forget gates of positions 0 to p; it never rises along p.
All inputs are finite; a program needn't handle non-finite values.
Results may differ from a plain program's by a relative error of at most 0.0095.
Values may be sent and summed in bfloat16 or wider, within the bound.
A program may use at most 64 MiB of HBM per device.

v0:
```python
import math

import jax
import jax.numpy as jnp
from jax import lax
from jax.sharding import Mesh
from jax.sharding import PartitionSpec as P

QUERY_HEADS = 8
KV_HEADS = 4
HEAD = 128
TOP_K = 2
EXP_SPAN = 4
EP = ("ep_0", "ep_1", "ep_2")


EPSILON = 1e-06


def from_everyone(x, axis):
    length = lax.axis_size(axis)
    return lax.all_to_all(jnp.broadcast_to(x[None], (length, *x.shape)), axis, 0, 0, tiled=True)


def of_everyone(x, axis):
    everything = from_everyone(x, axis)
    return jnp.sum(everything.astype(jnp.float32), axis=0)


def side_by_side(arrays, axis, dim, along):
    columns = [a.reshape(*a.shape[:along], -1) for a in arrays]
    both = jnp.concatenate(columns, axis=along)
    filled, at, outs = (lax.all_gather(both, axis, axis=dim, tiled=True), 0, [])
    for a, column in zip(arrays, columns):
        slab = filled[..., at : at + column.shape[along]]
        outs.append(slab.reshape(*slab.shape[:along], *a.shape[along:]))
        at += column.shape[along]
    return tuple(outs)


def in_one(arrays, axis):
    ends = [0]
    for a in arrays:
        ends.append(ends[-1] + a.size)
    subtotal = lax.psum(jnp.concatenate([a.ravel() for a in arrays]), axis)
    return tuple((subtotal[b:e].reshape(a.shape) for a, b, e in zip(arrays, ends, ends[1:])))


def cut_along(x, dim, length):
    lengths = x.shape
    blocks = x.reshape(*lengths[:dim], length, lengths[dim] // length, *lengths[dim + 1 :])
    return jnp.moveaxis(blocks, dim, 0)


def summed_on_arrival(x, axis, dim):
    length = lax.axis_size(axis)
    blocks = lax.all_to_all(cut_along(x, dim, length), axis, 0, 0, tiled=True)
    return jnp.sum(blocks.astype(jnp.float32), axis=0)


def sum_in_two_steps(x, axes, dim):
    far, near = axes
    own = summed_on_arrival(cut_along(x, dim, lax.axis_size(far)), near, dim + 1)
    return jnp.sum(
        lax.all_to_all(own.astype(jnp.bfloat16), far, 0, 0, tiled=True).astype(jnp.float32), axis=0
    )


def slot_table(route_block, expert_ids, capacity):
    blocks = route_block.shape[0]
    flat_routes = route_block.reshape(blocks, 1, -1)
    matched = (flat_routes == expert_ids.reshape(1, -1, 1)).astype(jnp.int32)
    ranking = jnp.cumsum(matched, axis=2) - 1
    slot_ids = jnp.arange(capacity, dtype=jnp.int32)
    taken = (matched[..., None] > 0) & (ranking[..., None] == slot_ids)
    table = jnp.swapaxes(taken, 2, 3).astype(jnp.float32)
    return table.reshape(
        blocks, expert_ids.shape[0], capacity, route_block.shape[1], route_block.shape[2]
    )


def attend(
    queries,
    new_keys,
    new_values,
    key_cache,
    value_cache,
    cum_gate,
    forget_logit,
    forget_bias,
    lengths,
):
    seqcount = queries.shape[0]
    kv_local = key_cache.shape[1]
    grouping = QUERY_HEADS // KV_HEADS
    heads_local = kv_local * grouping
    scale_factor = 1.0 / math.sqrt(HEAD)
    query_float = queries.astype(jnp.float32).reshape(seqcount, kv_local, grouping, HEAD)
    scores = jnp.einsum("sgjd,sgpd->sgjp", query_float, key_cache.astype(jnp.float32))
    scores = scores.reshape(seqcount, heads_local, -1) * scale_factor
    own_score = jnp.einsum(
        "sgjd,sgd->sgj", query_float, new_keys.astype(jnp.float32).reshape(seqcount, kv_local, HEAD)
    )
    own_score = own_score.reshape(seqcount, heads_local) * scale_factor
    log_forget = jax.nn.log_sigmoid(forget_logit + forget_bias)
    position = jnp.arange(cum_gate.shape[2], dtype=jnp.int32)
    latest = jnp.sum(jnp.where(position == (lengths - 1)[:, None, None], cum_gate, 0.0), axis=2)
    scores = scores + (latest + log_forget)[:, :, None] - cum_gate
    visible = position[None, None, :] < lengths[:, None, None]
    scores = jnp.where(visible, scores, -jnp.inf)
    highest = jnp.maximum(jnp.max(scores, axis=2), own_score)
    weights_past = jnp.exp(scores - highest[:, :, None])
    weight_own = jnp.exp(own_score - highest)
    totals = jnp.sum(weights_past, axis=2) + weight_own
    probs_past = (weights_past / totals[:, :, None]).astype(jnp.bfloat16)
    prob_own = (weight_own / totals).astype(jnp.bfloat16)
    mixed = jnp.einsum(
        "sgjp,sgpd->sgjd",
        probs_past.astype(jnp.float32).reshape(seqcount, kv_local, grouping, -1),
        value_cache.astype(jnp.float32),
    )
    mixed = mixed + prob_own.astype(jnp.float32).reshape(
        seqcount, kv_local, grouping, 1
    ) * new_values.astype(jnp.float32).reshape(seqcount, kv_local, 1, HEAD)
    return mixed.reshape(seqcount, heads_local * HEAD).astype(jnp.bfloat16)


def body(
    resid,
    queries,
    new_keys,
    new_values,
    key_cache,
    value_cache,
    cum_gate,
    forget_logit,
    forget_bias,
    lengths,
    out_weight,
    norm_gain,
    mix_vector,
    routes,
    route_weight,
    expert_gate,
    expert_up,
    expert_down,
    dense_gate,
    dense_up,
    dense_down,
):
    attended = attend(
        queries,
        new_keys,
        new_values,
        key_cache,
        value_cache,
        cum_gate,
        forget_logit,
        forget_bias,
        lengths,
    )
    head_part = jnp.dot(attended, out_weight, preferred_element_type=jnp.float32)
    projected = (
        of_everyone(head_part.astype(jnp.bfloat16), "tp").astype(jnp.float32).astype(jnp.bfloat16)
    )
    state_full = resid.astype(jnp.float32) + projected.astype(jnp.float32)
    inverse = lax.rsqrt(jnp.mean(state_full * state_full, axis=1) + EPSILON)
    scaled_full = state_full * norm_gain
    gate = jax.nn.sigmoid(inverse * jnp.sum(scaled_full * mix_vector.astype(jnp.float32), axis=1))
    channel_width = resid.shape[1] // lax.axis_size("tp")
    offset = lax.axis_index("tp") * channel_width
    state = lax.dynamic_slice_in_dim(state_full, offset, channel_width, 1)
    normed = (
        lax.dynamic_slice_in_dim(scaled_full, offset, channel_width, 1) * inverse[:, None]
    ).astype(jnp.bfloat16)
    ep_count = lax.axis_size(EP)
    tokens = resid.shape[0]
    experts = ep_count // EXP_SPAN
    capacity = min(tokens, 2 * ((tokens * TOP_K + experts - 1) // experts))
    w_gate = expert_gate[0]
    w_up = expert_up[0]
    w_down = expert_down[0]
    rows_all, routes_all, weights_all, gates_all = (
        lax.all_gather(normed, EP, axis=0, tiled=True),
        lax.all_gather(routes, EP, axis=0, tiled=True),
        *tuple(
            (
                part.astype(jnp.float32)
                for part in side_by_side(
                    (route_weight.astype(jnp.bfloat16), gate.astype(jnp.bfloat16)), EP, 0, 1
                )
            )
        ),
    )
    expert_id = lax.axis_index(EP) // EXP_SPAN
    table = slot_table(routes_all.reshape(ep_count, tokens, TOP_K), expert_id.reshape(1), capacity)[
        :, 0
    ]
    picked = jnp.sum(table, axis=3).astype(jnp.bfloat16)
    chosen = jnp.einsum(
        "bct,btd->bcd",
        picked,
        rows_all.reshape(ep_count, tokens, -1),
        preferred_element_type=jnp.float32,
    ).astype(jnp.bfloat16)
    chosen = chosen.reshape(ep_count * capacity, -1)
    expert_g, expert_u, dense_g, dense_u = tuple(
        (
            part.astype(jnp.float32)
            for part in in_one(
                (
                    jnp.dot(chosen, w_gate, preferred_element_type=jnp.float32).astype(
                        jnp.bfloat16
                    ),
                    jnp.dot(chosen, w_up, preferred_element_type=jnp.float32).astype(jnp.bfloat16),
                    jnp.dot(rows_all, dense_gate, preferred_element_type=jnp.float32).astype(
                        jnp.bfloat16
                    ),
                    jnp.dot(rows_all, dense_up, preferred_element_type=jnp.float32).astype(
                        jnp.bfloat16
                    ),
                ),
                "tp",
            )
        )
    )
    expert_hidden = (jax.nn.silu(expert_g) * expert_u).astype(jnp.bfloat16)
    outputs = jnp.dot(expert_hidden, w_down, preferred_element_type=jnp.float32)
    outputs = outputs.reshape(ep_count, capacity, -1)
    routed_all = jnp.einsum(
        "bctk,btk,bcd->btd",
        table,
        weights_all.reshape(ep_count, tokens, TOP_K),
        outputs,
        precision=lax.Precision.HIGHEST,
    ).reshape(ep_count * tokens, -1)
    dense_hidden = (jax.nn.silu(dense_g) * dense_u).astype(jnp.bfloat16)
    dense_part = jnp.dot(dense_hidden, dense_down, preferred_element_type=jnp.float32)
    combined = sum_in_two_steps(
        (dense_part * gates_all[:, None] + routed_all).astype(jnp.bfloat16),
        (("ep_0", "ep_1"), "ep_2"),
        0,
    )
    result = state + combined
    return result.astype(jnp.bfloat16)


def solution(mesh):
    torus = Mesh(mesh.devices.reshape(8, 8, 2, mesh.shape["tp"]), ("ep_0", "ep_1", "ep_2", "tp"))
    return jax.shard_map(
        body,
        mesh=torus,
        in_specs=(
            P(EP, None),
            P(EP, "tp"),
            P(EP, "tp"),
            P(EP, "tp"),
            P(EP, "tp", None, None),
            P(EP, "tp", None, None),
            P(EP, "tp", None),
            P(EP, "tp"),
            P("tp"),
            P(EP),
            P("tp", None),
            P(),
            P(),
            P(EP, None),
            P(EP, None),
            P(EP, "tp", None),
            P(EP, "tp", None),
            P(EP, None, "tp"),
            P("tp", EP),
            P("tp", EP),
            P(EP, "tp"),
        ),
        out_specs=P(EP, "tp"),
        check_vma=False,
    )
```

profile of v0, /device:TPU:1, one launch (start us, length us, event | category | flops | bytes accessed | tf_op | source)
XLA Modules:
  0.0 260.7 jit_solution(11100875189433785569)
XLA Ops:
  12.1 1.7 fusion.30
  14.0 1.5 fusion.4
  16.6 4.8 %all-to-all-start = ((bf16[4,16,2048]{2,1,0:T(8,128)(2,1)}), bf16[4,16,2048]{2,1,0:T(8,128)(2,1)S(1)}, u32[]{:S(2)}, u32[]{:S(2)}) async-start(bf16[4,16,2048]{2,1,0:T(8,128)(2,1)} %broadcast_in_dim.26), calls=%async_computation | async-start | bytes 524288 | tf_op jit(solution)/shard_map/all_to_all | solution.py:22
  21.4 5.5 %all-to-all-done = bf16[4,16,2048]{2,1,0:T(8,128)(2,1)S(1)} async-done(((bf16[4,16,2048]{2,1,0:T(8,128)(2,1)}), bf16[4,16,2048]{2,1,0:T(8,128)(2,1)S(1)}, u32[]{:S(2)}, u32[]{:S(2)}) %all-to-all-start) | async-done | bytes 262176 | tf_op jit(solution)/shard_map/all_to_all | solution.py:22
  29.1 59.4 %all-gather = s32[128,16,2]{1,2,0:T(2,128)S(1)} all-gather(s32[1,16,2]{1,2,0:T(2,128)S(1)} %bitcast.77), channel_id=1, replica_groups=mesh['ep_0'=8,'ep_1'=8,'ep_2'=2,'tp'=4] {'ep_0','ep_1','ep_2'}, dimensions={0}, use_global_device_ids=true | all-gather | bytes 16512 | tf_op jit(solution)/shard_map/all_gather | solution.py:185
  88.9 28.0 %all-gather.4.cloned.1.call-done = bf16[2048,512]{1,0:T(8,128)(2,1)} async-done(((bf16[16,512]{1,0:T(8,128)(2,1)}), bf16[2048,512]{1,0:T(8,128)(2,1)}) %all-gather.4.cloned.1.call-update) | async-done | bytes 2097168 | tf_op jit(solution)/shard_map/all_gather | solution.py:184
  116.9 2.0 convolution_convert_fusion.5
  119.0 2.4 convolution_convert_fusion.3
  121.4 2.1 reshape.285
  123.5 2.3 convolution_convert_fusion.4
  125.8 2.1 reshape.284
  129.6 2.4 reshape.286
  131.9 2.0 convolution_convert_fusion
  135.8 2.1 pad_maximum_fusion
  138.0 48.9 %all-gather.1 = bf16[128,16,3]{1,2,0:T(4,128)(2,1)S(1)} all-gather(bf16[1,16,3]{1,2,0:T(4,128)(2,1)S(1)} %maximum_bitcast_fusion), channel_id=1, replica_groups=mesh['ep_0'=8,'ep_1'=8,'ep_2'=2,'tp'=4] {'ep_0','ep_1','ep_2'}, dimensions={0}, use_global_device_ids=true | all-gather | bytes 12384 | tf_op jit(solution)/shard_map/all_gather | solution.py:33
  189.0 1.2 slice_convert_fusion.1
  190.9 1.6 slice_convert_fusion.3
  193.2 1.6 reshape.292
  194.8 1.5 fusion.7
  196.3 4.9 %fusion.11 = f32[128,16,512]{2,1,0:T(8,128)S(1)} fusion(f32[128,16,2]{1,2,0:T(2,128)} %copy.82, f32[128,2,512]{2,0,1:T(8,128)S(1)} %fusion.7), kind=kOutput, calls=%fused_computation.25 | convolution fusion | flops 25165824 | bytes 4734976 | tf_op jit(solution)/shard_map/bctk,btk,bcd->btd/dot_general | solution.py:230
  202.1 7.7 %all_to_all.15 = bf16[2,64,16,512]{3,2,1,0:T(8,128)(2,1)S(1)} all-to-all(bf16[2,64,16,512]{3,2,1,0:T(8,128)(2,1)S(1)} %bitcast.69), channel_id=1, replica_groups=mesh['ep_0'=8,'ep_1'=8,'ep_2'=2,'tp'=4] {'ep_2'}, dimensions={0} | all-to-all | bytes 4194304 | tf_op jit(solution)/shard_map/all_to_all | solution.py:57
  209.8 1.7 reduce_sum.84
  211.5 40.8 %all_to_all.16 = bf16[64,16,512]{2,1,0:T(8,128)(2,1)S(1)} all-to-all(bf16[64,16,512]{2,1,0:T(8,128)(2,1)} %reduce_sum.84), channel_id=1, replica_groups=mesh['ep_0'=8,'ep_1'=8,'ep_2'=2,'tp'=4] {'ep_0','ep_1'}, dimensions={0} | all-to-all | bytes 2097152 | tf_op jit(solution)/shard_map/all_to_all | solution.py:65
  252.5 1.4 add_convert_fusion
  (80 shorter events, 17.4 us)
Async XLA Ops:
  6.5 9.0 %copy-start = (bf16[256,2048]{1,0:T(8,128)(2,1)S(1)}, bf16[256,2048]{1,0:T(8,128)(2,1)}, u32[]{:S(2)}) copy-start(bf16[256,2048]{1,0:T(8,128)(2,1)} %param.31) | copy-start | bytes 3145732
  12.1 9.3 %copy-start.7 = (bf16[2048]{0:T(1024)(128)(2,1)S(1)}, bf16[2048]{0:T(1024)(128)(2,1)}, u32[]{:S(2)}) copy-start(bf16[2048]{0:T(1024)(128)(2,1)} %param.33) | copy-start | bytes 12292
  13.8 13.1 %copy-start.3 = (bf16[16,2048]{1,0:T(8,128)(2,1)S(1)}, bf16[16,2048]{1,0:T(8,128)(2,1)}, u32[]{:S(2)}) copy-start(bf16[16,2048]{1,0:T(8,128)(2,1)} %param.21) | copy-start | bytes 196612
  13.8 13.2 %copy-start.6 = (f32[2048]{0:T(1024)S(1)}, f32[2048]{0:T(1024)}, u32[]{:S(2)}) copy-start(f32[2048]{0:T(1024)} %param.32) | copy-start | bytes 24580
  13.8 15.3 %copy-start.9 = (s32[16,2]{0,1:T(2,128)S(1)}, s32[16,2]{0,1:T(2,128)}, u32[]{:S(2)}) copy-start(s32[16,2]{0,1:T(2,128)} %param.34) | copy-start | bytes 388
  16.6 10.4 %all-to-all-start = ((bf16[4,16,2048]{2,1,0:T(8,128)(2,1)}), bf16[4,16,2048]{2,1,0:T(8,128)(2,1)S(1)}, u32[]{:S(2)}, u32[]{:S(2)}) async-start(bf16[4,16,2048]{2,1,0:T(8,128)(2,1)} %broadcast_in_dim.26), calls=%async_computation | async-start | bytes 524288 | tf_op jit(solution)/shard_map/all_to_all | solution.py:22
  21.4 95.5 %all-gather.4.cloned.1.call-start = ((), (), s32[]{:S(2)}) async-start(), calls=%async_computation.3 | async-start | bytes 2113536 | tf_op jit(solution)/shard_map/all_gather | solution.py:184
  29.0 160.0 %all-reduce.2.cloned.1.call-start = ((), (), s32[]{:S(2)}) async-start(), calls=%async_computation.4 | async-start | bytes 1966080 | tf_op jit(solution)/shard_map/psum | solution.py:45
  119.0 8.9 %copy-start.1 = (bf16[2048,512]{1,0:T(8,128)(2,1)S(1)}, bf16[2048,512]{1,0:T(8,128)(2,1)}, u32[]{:S(2)}) copy-start(bf16[2048,512]{1,0:T(8,128)(2,1)} %all-gather.4.cloned.1.call-done) | copy-start | bytes 6291460
  119.0 8.9 %copy-start.4 = (bf16[512,24]{0,1:T(8,128)(2,1)S(1)}, bf16[512,24]{0,1:T(8,128)(2,1)}, u32[]{:S(2)}) copy-start(bf16[512,24]{0,1:T(8,128)(2,1)} %param.39) | copy-start | bytes 73732
  129.6 6.3 %copy-start.2 = (bf16[196608]{0:T(1024)(128)(2,1)S(1)}, bf16[196608]{0:T(1024)(128)(2,1)}, u32[]{:S(2)}) copy-start(bf16[196608]{0:T(1024)(128)(2,1)} %reshape.285) | copy-start | bytes 1179652
  134.0 4.0 %copy-start.10 = (f32[16,2]{0,1:T(2,128)S(1)}, f32[16,2]{0,1:T(2,128)}, u32[]{:S(2)}) copy-start(f32[16,2]{0,1:T(2,128)} %param.35) | copy-start | bytes 388
  134.0 4.0 %copy-start.8 = (bf16[16,1]{0,1:T(2,128)(2,1)S(1)}, bf16[16,1]{0,1:T(2,128)(2,1)}, u32[]{:S(2)}) copy-start(bf16[16,1]{0,1:T(2,128)(2,1)} %get-tuple-element.16) | copy-start | bytes 100
  196.3 4.9 %copy-start.5 = (bf16[24,512]{1,0:T(8,128)(2,1)S(1)}, bf16[24,512]{1,0:T(8,128)(2,1)}, u32[]{:S(2)}) copy-start(bf16[24,512]{1,0:T(8,128)(2,1)} %param.41) | copy-start | bytes 73732
Sparse Core Ops, SparseCore 0:
  29.1 87.7 all-gather.3
  138.1 50.9 all-reduce.1
where the time goes:
time: 263 us; the launch traced here: 261 us
  blocking collectives  157 us (60%)
  waiting for transfers between devices  34.5 us (13%)
  matrix products  20.7 us (8%)
  local copies, waits for them, and re-layouts  15.3 us (6%)
  other arithmetic  14.8 us (6%)
  between operations  13.8 us (5%)
  starting transfers between devices  4.87 us (2%)
    all_gather x1, blocking collectives, body(): lax.all_gather(routes, EP, axis=0, tiled=True)  59.4 us
    all_gather x1, blocking collectives, side_by_side(): filled, at, outs = (lax.all_gather(both, axis, axis=dim, tiled=True), 0, [])  48.9 us
    all_to_all x1, blocking collectives, sum_in_two_steps(): lax.all_to_all(own.astype(jnp.bfloat16), far, 0, 0, tiled=True)  40.8 us
    all_gather x1, waiting for transfers between devices, body(): lax.all_gather(normed, EP, axis=0, tiled=True)  28 us
    all_to_all x1, blocking collectives, summed_on_arrival(): blocks = lax.all_to_all(cut_along(x, dim, length), axis, 0, 0, tiled=True)  7.68 us
    reshape x4, local copies, waits for them, and re-layouts, in_one(): subtotal = lax.psum(jnp.concatenate([a.ravel() for a in arrays]), axis)  7.22 us
    all_to_all x1, waiting for transfers between devices, from_everyone(): lax.all_to_all(jnp.broadcast_to(x[None], (length, *x.shape)), axis, 0, 0,...  5.52 us
  transfers between devices with their start and end apart: 3, of which 3 were waited for; matrix products, arithmetic and copies ran while one was open for 1% of the time, Pallas kernels for 0%

commit v1 on v0

v1 whole, which is shorter than its diff:
```python
import functools
import math

import jax
import jax.numpy as jnp
from jax import lax
from jax.experimental import pallas as pl
from jax.experimental.pallas import tpu as pltpu
from jax.sharding import PartitionSpec as P

HEAD = 128
EPSILON = 1e-06
NC = 2
NY = 8
F32 = jnp.float32
BF16 = jnp.bfloat16


def dot(a, b):
    return jnp.dot(a, b, preferred_element_type=F32)


def dot_t(a, b):
    return lax.dot_general(a, b, (((1,), (1,)), ((), ())), preferred_element_type=F32)


def kernel(
    dims,
    resid_ref,
    q_ref,
    nk_ref,
    nv_ref,
    bias_ref,
    codes_ref,
    gm_ref,
    k_hbm,
    v_hbm,
    wo_hbm,
    wg_hbm,
    wu_hbm,
    wd_hbm,
    dg_hbm,
    du_hbm,
    dd_hbm,
    out_ref,
    k_v,
    v_v,
    wo_v,
    wg_v,
    wu_v,
    wd_v,
    dg_v,
    du_v,
    dd_v,
    ct,
    dw,
    xbuf,
    st,
    rows,
    pk,
    wmat,
    disp,
    er,
    psend,
    prec,
    hid,
    dacc,
    ret,
    rb,
    csend,
    cb,
    lsem,
    x_s,
    x_r,
    c_s,
    c_r,
    w_s,
    w_r,
    y_s,
    y_r,
    f_s,
    f_r,
    z_s,
    z_r,
    g_s,
    g_r,
    p_s,
    p_r,
    h_s,
    h_r,
    o_s,
    o_r,
    b_s,
    b_r,
):
    NX, NZ, S, SLOTS, DX, CW, NCH, FD, FDP = dims
    NQ = NY * NC // 4
    ep = lax.axis_index("ep")
    t = lax.axis_index("tp")
    c = lax.rem(ep, NC)
    y = lax.rem(ep // NC, NY)
    z = ep // (NC * NY)
    q = y // 2
    o = 1 - c

    def dev(zz, yy, cc, xx):
        return ((zz * NY + yy) * NC + cc, xx)

    def remote(src, dst, ss, rs, where):
        d = pltpu.make_async_remote_copy(
            src_ref=src,
            dst_ref=dst,
            send_sem=ss,
            recv_sem=rs,
            device_id=where,
            device_id_type=pl.DeviceIdType.MESH,
        )
        d.start()
        sent.append(d)
        return d

    sent = []
    xs = [lax.rem(t + d, NX) for d in range(NX)]
    xb = [lax.rem(t + NX - d, NX) for d in range(NX)]
    ys = [lax.rem(y + d, NY) for d in range(NY)]
    yb = [lax.rem(y + NY - d, NY) for d in range(NY)]
    zs = [lax.rem(z + d, NZ) for d in range(NZ)]
    zb = [lax.rem(z + NZ - d, NZ) for d in range(NZ)]

    def order(n):
        return sorted(range(1, n), key=lambda d: (min(d, n - d), d))

    group = [(dc, dy) for dy in [0] + order(NY) for dc in range(NC) if dc + dy > 0]

    loads = {}
    for i, (name, src, dst) in enumerate(
        (
            ("dg", dg_hbm, dg_v),
            ("du", du_hbm, du_v),
            ("dd", dd_hbm, dd_v),
            ("k", k_hbm, k_v),
            ("v", v_hbm, v_v),
            ("wo", wo_hbm, wo_v),
            ("wg", wg_hbm, wg_v),
            ("wu", wu_hbm, wu_v),
            ("wd", wd_hbm, wd_v),
        )
    ):
        loads[name] = pltpu.make_async_copy(src, dst, lsem.at[i])
        loads[name].start()

    barrier = pltpu.get_barrier_semaphore()
    peers = [dev(z, y, c, xs[d]) for d in range(1, NX)]
    peers += [dev(z, ys[dy], (c if dc == 0 else o), t) for dc, dy in group]
    peers += [dev(zs[d], y, c, t) for d in range(1, NZ)]
    for p in peers:
        pl.semaphore_signal(barrier, inc=1, device_id=p, device_id_type=pl.DeviceIdType.MESH)

    loads["dg"].wait()
    loads["du"].wait()
    loads["dd"].wait()
    dw[z] = jnp.concatenate(
        [
            dg_v[...].astype(F32).T,
            du_v[...].astype(F32).T,
            dd_v[...].astype(F32),
            jnp.zeros((dw.shape[1] - 3 * FD, DX), F32),
        ],
        axis=0,
    ).astype(BF16)
    ct[c, y] = codes_ref[...]

    pl.semaphore_wait(barrier, len(peers))

    c_cp = {}
    for dc, dy in group:
        i = dc * NY + dy
        c_cp[i] = remote(
            codes_ref,
            ct.at[c, y],
            c_s.at[i],
            c_r.at[i],
            dev(z, ys[dy], (c if dc == 0 else o), t),
        )
    w_cp = {}
    for d in order(NZ):
        w_cp[d] = remote(dw.at[z], dw.at[z], w_s.at[d], w_r.at[d], dev(zs[d], y, c, t))

    loads["k"].wait()
    qq = q_ref[...]
    q2 = jnp.concatenate([qq[:, :HEAD], qq[:, HEAD:]], axis=0)
    rowid = lax.rem(lax.broadcasted_iota(jnp.int32, (2 * S, SLOTS), 0), S)
    raw = jnp.zeros((2 * S, SLOTS), F32)
    for s in range(S):
        part = dot_t(q2, k_v[s * SLOTS : (s + 1) * SLOTS, :])
        raw = jnp.where(rowid == s, part, raw)
    scale = 1.0 / math.sqrt(HEAD)
    scores = raw * scale + bias_ref[...]
    nk = nk_ref[...].astype(F32)
    nv = nv_ref[...].astype(F32)
    own = jnp.sum(q2.astype(F32) * jnp.concatenate([nk, nk], axis=0), axis=1, keepdims=True) * scale
    top = jnp.maximum(jnp.max(scores, axis=1, keepdims=True), own)
    past = jnp.exp(scores - top)
    wown = jnp.exp(own - top)
    total = jnp.sum(past, axis=1, keepdims=True) + wown
    probs = (past / total).astype(BF16).astype(F32)
    pown = (wown / total).astype(BF16).astype(F32)
    loads["v"].wait()
    mixed = pown * jnp.concatenate([nv, nv], axis=0)
    for s in range(S):
        mixed = mixed + dot(
            jnp.where(rowid == s, probs, 0.0).astype(BF16), v_v[s * SLOTS : (s + 1) * SLOTS, :]
        )
    mixed = mixed.astype(BF16)
    attended = jnp.concatenate([mixed[:S], mixed[S:]], axis=1)
    loads["wo"].wait()
    for j in range(NX):
        xbuf[t, j] = dot(attended, wo_v[:, j * DX : (j + 1) * DX]).astype(BF16)
    x_cp = {}
    for d in order(NX):
        x_cp[d] = remote(xbuf.at[t], xbuf.at[t], x_s.at[d], x_r.at[d], dev(z, y, c, xs[d]))

    for dc, dy in group:
        c_cp[dc * NY + dy].wait_recv()
    acode = [jnp.sum(ct[i], axis=0) for i in range(NC)]
    mine = jnp.sum(ct[c], axis=0)
    nslot = 2 * NY
    npick = NZ * nslot
    ntok = NY * S
    ii = lax.broadcasted_iota(jnp.int32, (npick, ntok), 0)
    tt = lax.broadcasted_iota(jnp.int32, (npick, ntok), 1)
    target = (2 * ((ii // nslot) * NQ + q) + lax.rem(ii // NY, 2) + 1).astype(F32)
    same = lax.rem(ii, NY) == tt // S
    hit = ((mine[0:1] == target) | (mine[1:2] == target)) & same
    pk[...] = jnp.where(hit, 1.0, 0.0).astype(BF16)
    nall = NC * npick
    ii = lax.broadcasted_iota(jnp.int32, (nall, NC * ntok), 0)
    tt = lax.broadcasted_iota(jnp.int32, (nall, NC * ntok), 1)
    target = (2 * ((ii // (NC * nslot)) * NQ + q) + lax.rem(ii // NY, 2) + 1).astype(F32)
    same = (lax.rem(ii, NY) == lax.rem(tt // S, NY)) & (lax.rem(ii // nslot, NC) == tt // ntok)
    allc = jnp.concatenate(acode, axis=1)
    wt = jnp.where((allc[0:1] == target) & same, allc[2:3], 0.0) + jnp.where(
        (allc[1:2] == target) & same, allc[3:4], 0.0
    )
    wt = wt.T
    whi = wt.astype(BF16)
    wmat[:, 0:nall] = whi
    wmat[:, nall : 2 * nall] = (wt - whi.astype(F32)).astype(BF16)

    for d in order(NX):
        x_cp[d].wait_recv()
    sumsq = jnp.zeros((S, 1), F32)
    gsum = jnp.zeros((S, 1), F32)
    for j in range(NX):
        proj = xbuf[0, j].astype(F32)
        for i in range(1, NX):
            proj = proj + xbuf[i, j].astype(F32)
        state = resid_ref[:, j * DX : (j + 1) * DX].astype(F32) + proj.astype(BF16).astype(F32)
        sumsq = sumsq + jnp.sum(state * state, axis=1, keepdims=True)
        scaled = state * gm_ref[0:1, j * DX : (j + 1) * DX]
        gsum = gsum + jnp.sum(scaled * gm_ref[1:2, j * DX : (j + 1) * DX], axis=1, keepdims=True)
        st[0, j] = state
        st[1, j] = scaled
    inverse = lax.rsqrt(sumsq / (NX * DX) + EPSILON)
    gate = 1.0 / (1.0 + jnp.exp(-(inverse * gsum)))
    ghi = gate.astype(BF16).astype(F32)
    lane = lax.broadcasted_iota(jnp.int32, (S, 128), 1)
    rows[c, y, :, 0:DX] = (st[1, t] * inverse).astype(BF16)
    rows[c, y, :, DX : DX + 128] = jnp.where(
        lane == 0, ghi, jnp.where(lane == 1, gate - ghi, 0.0)
    ).astype(BF16)

    y_cp, f_cp = {}, {}
    for d in order(NY):
        y_cp[d] = remote(
            rows.at[c, y], rows.at[c, y], y_s.at[d], y_r.at[d], dev(z, ys[d], c, t)
        )
    f_cp[0] = remote(rows.at[c, y], rows.at[c, y], f_s.at[0], f_r.at[0], dev(z, y, o, t))
    for d in order(NY):
        y_cp[d].wait_recv()
        f_cp[d] = remote(
            rows.at[c, yb[d]], rows.at[c, yb[d]], f_s.at[d], f_r.at[d], dev(z, y, o, t)
        )

    own_rows = rows[c, :, :, 0:DX].reshape(ntok, DX)
    disp[...] = dot(pk[...], own_rows).astype(BF16).reshape(NZ, nslot, DX)
    er[c * NZ + z] = disp[z]
    z_cp, g_cp = {}, {}
    for d in order(NZ):
        z_cp[d] = remote(
            disp.at[zs[d]], er.at[c * NZ + z], z_s.at[d], z_r.at[d], dev(zs[d], y, c, t)
        )
    g_cp[0] = remote(
        disp.at[z], er.at[c * NZ + z], g_s.at[0], g_r.at[0], dev(z, y, o, t)
    )

    for d in range(NY):
        f_cp[d].wait_recv()
    for d in order(NZ):
        w_cp[d].wait_recv()
    dwf = dw[...].astype(F32)
    fill = jnp.zeros((FDP - NZ * FD, DX), F32)
    dgw, duw, ddw = [
        jnp.concatenate([dwf[:, i * FD : (i + 1) * FD].reshape(NZ * FD, DX), fill], axis=0).astype(
            BF16
        )
        for i in range(3)
    ]
    ntoks = NC * ntok
    chunk = ntoks // NX
    all_rows = rows[:, :, :, 0:DX].reshape(ntoks, DX)
    psend[NCH, :, :, 0:CW] = dot_t(all_rows, dgw).astype(BF16).reshape(NX, chunk, CW)
    psend[NCH, :, :, CW : 2 * CW] = dot_t(all_rows, duw).astype(BF16).reshape(NX, chunk, CW)
    p_cp, h_cp = {}, {}

    def scatter(j):
        for d in order(NX)[::-1]:
            p_cp[j, d] = remote(
                psend.at[j, xs[d]],
                prec.at[j, d - 1],
                p_s.at[j, d - 1],
                p_r.at[j, d - 1],
                dev(z, y, c, xs[d]),
            )

    def hidden(j):
        acc = psend[j, t].astype(F32)
        for d in order(NX):
            p_cp[j, d].wait_recv()
        for d in range(1, NX):
            acc = acc + prec[j, d - 1].astype(F32)
        g, u = acc[:, :CW], acc[:, CW:]
        hid[j, t] = (g / (1.0 + jnp.exp(-g)) * u).astype(BF16)
        for d in order(NX)[::-1]:
            h_cp[j, d] = remote(
                hid.at[j, t],
                hid.at[j, t],
                h_s.at[j, d - 1],
                h_r.at[j, d - 1],
                dev(z, y, c, xs[d]),
            )

    def gathered(j):
        for d in order(NX):
            h_cp[j, d].wait_recv()
        return hid[j].reshape(ntoks, CW)

    scatter(NCH)

    for d in order(NZ):
        z_cp[d].wait_recv()
        g_cp[d] = remote(
            er.at[c * NZ + zb[d]],
            er.at[c * NZ + zb[d]],
            g_s.at[d],
            g_r.at[d],
            dev(z, y, o, t),
        )
    hidden(NCH)
    loads["wg"].wait()
    loads["wu"].wait()
    for d in range(NZ):
        g_cp[d].wait_recv()
    picked = er[...].reshape(nall, DX)
    for j in range(NCH):
        psend[j, :, :, 0:CW] = (
            dot(picked, wg_v[:, j * CW : (j + 1) * CW]).astype(BF16).reshape(NX, chunk, CW)
        )
        psend[j, :, :, CW : 2 * CW] = (
            dot(picked, wu_v[:, j * CW : (j + 1) * CW]).astype(BF16).reshape(NX, chunk, CW)
        )
        scatter(j)
    gates = rows[:, :, :, DX : DX + 128].reshape(ntoks, 128)
    gates = gates[:, 0:1].astype(F32) + gates[:, 1:2].astype(F32)
    dacc[...] = gates * dot(gathered(NCH), ddw)
    for j in range(NCH):
        hidden(j)
    loads["wd"].wait()
    outs = dot(gathered(0), wd_v[0:CW, :])
    for j in range(1, NCH):
        outs = outs + dot(gathered(j), wd_v[j * CW : (j + 1) * CW, :])
    outs = outs.astype(BF16)

    for zz in range(NZ):
        for cc in range(NC):
            at = (cc * NZ + zz) * nslot
            ret[zz, cc] = outs[at : at + nslot]
    rb[z] = ret[z]
    o_cp = {}
    for d in order(NZ)[::-1]:
        o_cp[d] = remote(ret.at[zs[d]], rb.at[z], o_s.at[d], o_r.at[d], dev(zs[d], y, c, t))
    for d in order(NZ):
        o_cp[d].wait_recv()
    back = rb[...].reshape(nall, DX)
    both = jnp.concatenate([back, back], axis=0)
    comb = dot(wmat[...], both) + dacc[...]
    csend[...] = comb.astype(BF16).reshape(NC, NY, S, DX)

    cb[c, y] = csend[c, y]
    b_cp = {}
    for dc, dy in group[::-1]:
        i = dc * NY + dy
        cc = c if dc == 0 else o
        b_cp[i] = remote(
            csend.at[cc, ys[dy]], cb.at[c, y], b_s.at[i], b_r.at[i], dev(z, ys[dy], cc, t)
        )
    for dc, dy in group:
        b_cp[dc * NY + dy].wait_recv()
    res = st[0, t]
    for cc in range(NC):
        for yy in range(NY):
            res = res + cb[cc, yy].astype(F32)
    out_ref[...] = res.astype(BF16)
    for d in sent:
        d.wait_send()


def body(
    resid,
    queries,
    new_keys,
    new_values,
    key_cache,
    value_cache,
    cum_gate,
    forget_logit,
    forget_bias,
    lengths,
    out_weight,
    norm_gain,
    mix_vector,
    routes,
    route_weight,
    expert_gate,
    expert_up,
    expert_down,
    dense_gate,
    dense_up,
    dense_down,
):
    NX = lax.axis_size("tp")
    n_ep = lax.axis_size("ep")
    NZ = n_ep // (NC * NY)
    S, D = resid.shape
    SLOTS = key_cache.shape[2]
    DX = D // NX
    FF = expert_gate.shape[2]
    FD = dense_gate.shape[1]
    CW = min(256, FF)
    NCH = FF // CW
    FDP = CW
    ep = lax.axis_index("ep")
    y = lax.rem(ep // NC, NY)

    position = jnp.arange(SLOTS, dtype=jnp.int32)
    lens = lengths[:, None, None]
    latest = jnp.sum(jnp.where(position == lens - 1, cum_gate, 0.0), axis=2)
    log_forget = jax.nn.log_sigmoid(forget_logit + forget_bias)
    bias = jnp.where(position < lens, (latest + log_forget)[:, :, None] - cum_gate, -jnp.inf)
    bias = jnp.swapaxes(bias, 0, 1).reshape(2 * S, SLOTS)

    earlier = jnp.arange(S)[None, :] < jnp.arange(S)[:, None]
    equal = routes[:, :, None, None] == routes[None, None, :, :]
    rank = jnp.sum(jnp.where(equal & earlier[:, None, :, None], 1, 0), axis=(2, 3))
    code = (2 * routes + rank + 1).astype(F32)
    four = jnp.concatenate([code.T, route_weight.T, jnp.zeros((4, S), F32)], axis=0)
    lane = jnp.arange(NY * S)
    codes = jnp.where(lane // S == y, jnp.tile(four, (1, NY)), 0.0)
    gm = jnp.stack([norm_gain, mix_vector.astype(F32)])

    dims = (NX, NZ, S, SLOTS, DX, CW, NCH, FD, FDP)
    nslot = 2 * NY
    npick = NZ * nslot
    ntok = NY * S
    DWR = -(-3 * FD // 16) * 16
    vm = pl.BlockSpec(memory_space=pltpu.VMEM)
    hb = pl.BlockSpec(memory_space=pl.ANY)
    dma = pltpu.SemaphoreType.DMA
    scratch = [
        pltpu.VMEM((S * SLOTS, HEAD), BF16),
        pltpu.VMEM((S * SLOTS, HEAD), BF16),
        pltpu.VMEM((2 * HEAD, D), BF16),
        pltpu.VMEM((DX, FF), BF16),
        pltpu.VMEM((DX, FF), BF16),
        pltpu.VMEM((FF, DX), BF16),
        pltpu.VMEM((DX, FD), BF16),
        pltpu.VMEM((DX, FD), BF16),
        pltpu.VMEM((FD, DX), BF16),
        pltpu.VMEM((NC, NY, 8, ntok), F32),
        pltpu.VMEM((NZ, DWR, DX), BF16),
        pltpu.VMEM((NX, NX, S, DX), BF16),
        pltpu.VMEM((2, NX, S, DX), F32),
        pltpu.VMEM((NC, NY, S, DX + 128), BF16),
        pltpu.VMEM((npick, ntok), BF16),
        pltpu.VMEM((NC * ntok, 2 * NC * npick), BF16),
        pltpu.VMEM((NZ, nslot, DX), BF16),
        pltpu.VMEM((NC * NZ, nslot, DX), BF16),
        pltpu.VMEM((NCH + 1, NX, NC * ntok // NX, 2 * CW), BF16),
        pltpu.VMEM((NCH + 1, NX - 1, NC * ntok // NX, 2 * CW), BF16),
        pltpu.VMEM((NCH + 1, NX, NC * ntok // NX, CW), BF16),
        pltpu.VMEM((NC * ntok, DX), F32),
        pltpu.VMEM((NZ, NC, nslot, DX), BF16),
        pltpu.VMEM((NZ, NC, nslot, DX), BF16),
        pltpu.VMEM((NC, NY, S, DX), BF16),
        pltpu.VMEM((NC, NY, S, DX), BF16),
        dma((9,)),
        dma((NX,)),
        dma((NX,)),
        dma((NC * NY,)),
        dma((NC * NY,)),
        dma((NZ,)),
        dma((NZ,)),
        dma((NY,)),
        dma((NY,)),
        dma((NY,)),
        dma((NY,)),
        dma((NZ,)),
        dma((NZ,)),
        dma((NZ,)),
        dma((NZ,)),
        dma((NCH + 1, NX - 1)),
        dma((NCH + 1, NX - 1)),
        dma((NCH + 1, NX - 1)),
        dma((NCH + 1, NX - 1)),
        dma((NZ,)),
        dma((NZ,)),
        dma((NC * NY,)),
        dma((NC * NY,)),
    ]
    return pl.pallas_call(
        functools.partial(kernel, dims),
        name="layer",
        out_shape=jax.ShapeDtypeStruct((S, DX), BF16),
        in_specs=[vm] * 7 + [hb] * 9,
        out_specs=vm,
        scratch_shapes=scratch,
        compiler_params=pltpu.CompilerParams(
            collective_id=0, has_side_effects=True, vmem_limit_bytes=56 * 1024 * 1024
        ),
    )(
        resid,
        queries,
        new_keys,
        new_values,
        bias,
        codes,
        gm,
        key_cache.reshape(S * SLOTS, HEAD),
        value_cache.reshape(S * SLOTS, HEAD),
        out_weight,
        expert_gate[0],
        expert_up[0],
        expert_down[0],
        dense_gate,
        dense_up,
        dense_down,
    )


def solution(mesh):
    return jax.shard_map(
        body,
        mesh=mesh,
        in_specs=(
            P("ep", None),
            P("ep", "tp"),
            P("ep", "tp"),
            P("ep", "tp"),
            P("ep", "tp", None, None),
            P("ep", "tp", None, None),
            P("ep", "tp", None),
            P("ep", "tp"),
            P("tp"),
            P("ep"),
            P("tp", None),
            P(),
            P(),
            P("ep", None),
            P("ep", None),
            P("ep", "tp", None),
            P("ep", "tp", None),
            P("ep", None, "tp"),
            P("tp", "ep"),
            P("tp", "ep"),
            P("ep", "tp"),
        ),
        out_specs=P("ep", "tp"),
        check_vma=False,
    )
```

time: 263 us -> 80.6 us (0.31)
  blocking collectives: 157 us -> 0 us
  Pallas kernels: 0 us -> 70.4 us
  waiting for transfers between devices: 34.5 us -> 0 us
  matrix products: 20.7 us -> 0 us
  between operations: 13.8 us -> 0.07 us
  other arithmetic: 14.8 us -> 1.91 us
  local copies, waits for them, and re-layouts: 15.3 us -> 7.72 us
  starting transfers between devices: 4.87 us -> 0 us
    all_gather x2 -> x0, blocking collectives: 108 us -> none  [the longest x1 59.4 us: body(): lax.all_gather(routes, EP, axis=0, tiled=True)]
    pallas_call x0 -> x1, Pallas kernels: none -> 70.4 us  [body(): pl.pallas_call(functools.partial(kernel, dims), name='layer', out_shape=j...]
    all_to_all x2 -> x0, blocking collectives: 48.4 us -> none  [the longest x1 40.8 us: sum_in_two_steps(): lax.all_to_all(own.astype(jnp.bfloat16), far, 0, 0, tiled=True)]
    all_gather x1 -> x0, waiting for transfers between devices: 28 us -> none  [body(): lax.all_gather(normed, EP, axis=0, tiled=True)]
    dot_general x12 -> x0, matrix products: 20.7 us -> none  [the longest x1 4.86 us: body(): jnp.einsum('bctk,btk,bcd->btd', table, weights_all.reshape(ep_count, toke...]
    reshape x6 -> x0, local copies, waits for them, and re-layouts: 7.43 us -> none  [the longest x4 7.22 us: in_one(): subtotal = lax.psum(jnp.concatenate([a.ravel() for a in arrays]), axis)]
    unnamed x24 -> x23, local copies, waits for them, and re-layouts: 0.26 us -> 6.79 us
    convert_element_type x10 -> x0, other arithmetic: 5.84 us -> none  [the longest x2 2.86 us: body(): part.astype(jnp.float32)]
  transfers between devices with their start and end apart: 3 -> 0, of which waited for: 3 -> 0; matrix products, arithmetic and copies ran while one was open for 1% -> 0% of each run, Pallas kernels for 0% -> 0%
where the time goes in v1:
time: 80.6 us; the launch traced here: 80.1 us
  Pallas kernels  70.4 us (87%)
  local copies, waits for them, and re-layouts  7.72 us (10%)
  other arithmetic  1.91 us (2%)
    pallas_call x1, Pallas kernels, body(): pl.pallas_call(functools.partial(kernel, dims), name='layer', out_shape=j...  70.4 us
    unnamed x23, local copies, waits for them, and re-layouts  6.79 us

profile of v1, /device:TPU:1, one launch (start us, length us, event | category | flops | bytes accessed | tf_op | source)
XLA Modules:
  0.0 80.1 jit_solution(2617112132491796489)
XLA Ops:
  0.0 0.6 copy-done.9
  0.7 0.1 pad.4.clone
  0.8 0.7 copy-done.3
  1.4 0.2 select_reduce_fusion
  1.6 0.7 copy-done.7
  2.3 0.1 maximum_maximum_fusion
  2.4 0.1 iota_compare_fusion
  2.5 0.1 select_reduce_fusion.1
  2.6 0.1 copy.40
  2.7 0.6 copy-done.6
  3.2 0.1 fusion.1
  3.3 0.1 iota_compare_fusion.1
  3.4 0.1 copy.41
  3.5 0.6 copy-done.5
  4.1 0.7 copy-done.4
  4.8 0.6 pad_maximum_fusion.gm_ref
  5.4 0.1 select_bitcast_fusion
  5.5 0.6 copy.42
  6.1 0.1 tile.10
  6.2 0.6 broadcast_select_fusion.codes_ref
  6.9 0.8 copy.43.dg_hbm
  7.6 0.8 copy.44.du_hbm
  8.4 70.4 %layer.1 = bf16[16,512]{1,0:T(8,128)(2,1)} custom-call(bf16[16,2048]{1,0:T(8,128)(2,1)} %resid_ref.1, bf16[16,256]{1,0:T(8,128)(2,1)} %q_ref.1, bf16[16,128]{1,0:T(8,128)(2,1)} %nk_ref.1, bf16[16,128]{1,0:T(8,128)(2,1)} %nv_ref.1, f32[32,256]{1,0:T(8,128)} %bitcast.18, f32[8,128]{1,0:T(8,128)} %broadcast_select_fusion.codes_ref, ...), custom_call_target="tpu_custom_call" | custom-call | tf_op jit(solution)/shard_map/layer/pallas_call | solution.py:530
  78.8 1.3 %copy.46 = bf16[16,512]{1,0:T(8,128)(2,1)} copy(bf16[16,512]{1,0:T(8,128)(2,1)} %layer.1) | data formatting | bytes 32768
  (21 shorter events, 0.1 us)
Async XLA Ops:
  0.0 2.5 %copy-start = (f32[16,2,256]{2,1,0:T(2,128)S(1)}, f32[16,2,256]{2,1,0:T(2,128)}, u32[]{:S(2)}) copy-start(f32[16,2,256]{2,1,0:T(2,128)} %param.27) | copy-start | bytes 98308
  0.0 0.7 copy-start.9
  0.8 0.7 copy-start.3
  1.6 0.7 copy-start.7
  2.6 0.7 copy-start.6
  2.6 0.7 copy-start.8
  3.4 0.7 copy-start.5
  4.1 0.7 copy-start.4
  6.1 0.7 copy-start.1
  6.9 0.8 copy-start.2

commit v2 on v1

v2 whole, which is shorter than its diff:
```python
import functools
import math

import jax
import jax.numpy as jnp
from jax import lax
from jax.experimental import pallas as pl
from jax.experimental.pallas import tpu as pltpu
from jax.sharding import PartitionSpec as P

HEAD = 128
EPSILON = 1e-06
NC = 2
NY = 8
F32 = jnp.float32
BF16 = jnp.bfloat16


def dot(a, b):
    return jnp.dot(a, b, preferred_element_type=F32)


def dot_t(a, b):
    return lax.dot_general(a, b, (((1,), (1,)), ((), ())), preferred_element_type=F32)


ARGS = (
    ("resid", "q", "nk", "nv", "cg", "fl", "fb", "len", "rt", "rw", "gain", "mix")
    + ("k", "v", "wo", "wg", "wu", "wd", "dg", "du", "dd")
)


def kernel(dims, *refs):
    h = dict(zip(ARGS, refs))
    out_ref = refs[len(ARGS)]
    rest = refs[len(ARGS) + 1 :]
    local = dict(zip(ARGS[:18], rest))
    (codes, ct, dw, xbuf, st, rows, gts, pk, wmat, disp, er, psend, prec, hid) = rest[18:32]
    (psd, prd, hdd, dacc, osend, orecv, ret, rb, csend, cb) = rest[32:42]
    (lsem, xq, cq, wq, vq, yq, tq, zq, gq, pq, hq, aq, eq, sq, oq, bq) = rest[42:]
    NX, NZ, S, SLOTS, DX, CW, NCH, FD = dims
    NQ = NY * NC // 4
    ep = lax.axis_index("ep")
    t = lax.axis_index("tp")
    c = lax.rem(ep, NC)
    y = lax.rem(ep // NC, NY)
    z = ep // (NC * NY)
    q = y // 2
    o = 1 - c

    def dev(zz, yy, cc, xx):
        return ((zz * NY + yy) * NC + cc, xx)

    def remote(src, dst, sems, i, where):
        d = pltpu.make_async_remote_copy(
            src_ref=src,
            dst_ref=dst,
            send_sem=sems.at[(0, *i)],
            recv_sem=sems.at[(1, *i)],
            device_id=where,
            device_id_type=pl.DeviceIdType.MESH,
        )
        d.start()
        sent.append(d)
        return d

    sent = []
    xs = [lax.rem(t + d, NX) for d in range(NX)]
    xb = [lax.rem(t + NX - d, NX) for d in range(NX)]
    ys = [lax.rem(y + d, NY) for d in range(NY)]
    yb = [lax.rem(y + NY - d, NY) for d in range(NY)]
    zs = [lax.rem(z + d, NZ) for d in range(NZ)]
    zb = [lax.rem(z + NZ - d, NZ) for d in range(NZ)]

    def order(n):
        return sorted(range(1, n), key=lambda d: (min(d, n - d), d))

    partner = dev(z, y, o, t)
    barrier = pltpu.get_barrier_semaphore()
    peers = [dev(z, y, c, xs[d]) for d in range(1, NX)]
    peers += [dev(z, ys[d], c, t) for d in range(1, NY)]
    peers += [dev(zs[d], y, c, t) for d in range(1, NZ)]
    peers.append(partner)
    for p in peers:
        pl.semaphore_signal(barrier, inc=1, device_id=p, device_id_type=pl.DeviceIdType.MESH)

    loads = {}
    targets = dict(local, dg=dw.at[c, z, 0], du=dw.at[c, z, 1], dd=dw.at[c, z, 2])
    first = ["q", "k", "len", "rt", "cg", "fl", "fb", "rw", "nk", "nv", "v", "wo"]
    first += ["resid", "gain", "mix"]
    for i, name in enumerate(first + [a for a in ARGS if a not in first]):
        loads[name] = pltpu.make_async_copy(h[name], targets[name], lsem.at[i])
        loads[name].start()

    def get(name):
        loads[name].wait()
        return local[name]

    tr = lax.broadcasted_iota(jnp.int32, (S, S), 0)
    tc = lax.broadcasted_iota(jnp.int32, (S, S), 1)

    def column(row):
        return jnp.sum(jnp.where(tr == tc, row, jnp.zeros_like(row)), axis=1, keepdims=True)

    rt = get("rt")[...].astype(F32)
    rw = get("rw")[...]
    lanes = lax.broadcasted_iota(jnp.int32, (S, NY * S), 1)
    place = lanes == y * S + lax.broadcasted_iota(jnp.int32, (S, NY * S), 0)
    for k in range(2):
        mine = column(rt[k : k + 1])
        rank = jnp.zeros((S, 1), F32)
        for i in range(2):
            taken = (rt[i : i + 1] == mine) & (tc < tr)
            rank = rank + jnp.sum(jnp.where(taken, 1.0, 0.0), axis=1, keepdims=True)
        code = 2.0 * mine + rank + 1.0
        codes[k : k + 1] = jnp.sum(jnp.where(place, code, 0.0), axis=0, keepdims=True)
        codes[2 + k : 3 + k] = jnp.sum(
            jnp.where(place, column(rw[k : k + 1]), 0.0), axis=0, keepdims=True
        )
    codes[4:8] = jnp.zeros((4, NY * S), F32)
    ct[y] = codes[...]

    lens = column(get("len")[...])
    cg_ref, fl_ref, fb_ref = get("cg"), get("fl"), get("fb")
    pos = lax.broadcasted_iota(jnp.int32, (S, SLOTS), 1)
    biases = []
    for j in range(2):
        cg = cg_ref[:, j, :]
        latest = jnp.sum(jnp.where(pos == lens - 1, cg, 0.0), axis=1, keepdims=True)
        pre = column(fl_ref[j : j + 1]) + fb_ref[0:1, j : j + 1]
        forget = jnp.minimum(pre, 0.0) - jnp.log(1.0 + jnp.exp(-jnp.abs(pre)))
        biases.append(jnp.where(pos < lens, latest + forget - cg, -jnp.inf))
    bias = jnp.concatenate(biases, axis=0)

    k_v = get("k")
    qq = get("q")[...]
    q2 = jnp.concatenate([qq[:, :HEAD], qq[:, HEAD:]], axis=0)
    rowid = lax.rem(lax.broadcasted_iota(jnp.int32, (2 * S, SLOTS), 0), S)
    raw = jnp.zeros((2 * S, SLOTS), F32)
    for s in range(S):
        part = dot_t(q2, k_v[s * SLOTS : (s + 1) * SLOTS, :])
        raw = jnp.where(rowid == s, part, raw)
    scale = 1.0 / math.sqrt(HEAD)
    scores = raw * scale + bias
    nk = get("nk")[...].astype(F32)
    nv = get("nv")[...].astype(F32)
    own = jnp.sum(q2.astype(F32) * jnp.concatenate([nk, nk], axis=0), axis=1, keepdims=True) * scale
    top = jnp.maximum(jnp.max(scores, axis=1, keepdims=True), own)
    past = jnp.exp(scores - top)
    wown = jnp.exp(own - top)
    total = jnp.sum(past, axis=1, keepdims=True) + wown
    probs = (past / total).astype(BF16).astype(F32)
    pown = (wown / total).astype(BF16).astype(F32)
    v_v = get("v")
    mixed = pown * jnp.concatenate([nv, nv], axis=0)
    for s in range(S):
        mixed = mixed + dot(
            jnp.where(rowid == s, probs, 0.0).astype(BF16), v_v[s * SLOTS : (s + 1) * SLOTS, :]
        )
    mixed = mixed.astype(BF16)
    attended = jnp.concatenate([mixed[:S], mixed[S:]], axis=1)
    wo_v = get("wo")
    for j in range(NX):
        xbuf[t, j] = dot(attended, wo_v[:, j * DX : (j + 1) * DX]).astype(BF16)
    pl.semaphore_wait(barrier, len(peers))
    x_cp, c_cp, w_cp = {}, {}, {}
    for d in order(NX):
        x_cp[d] = remote(xbuf.at[t], xbuf.at[t], xq, (d,), dev(z, y, c, xs[d]))
    for d in order(NY):
        c_cp[d] = remote(codes, ct.at[y], cq, (d,), dev(z, ys[d], c, t))
    for name in ("dg", "du", "dd"):
        loads[name].wait()
    for d in order(NZ):
        w_cp[d] = remote(dw.at[c, z], dw.at[c, z], wq, (d,), dev(zs[d], y, c, t))

    for d in order(NY):
        c_cp[d].wait_recv()
    mine = jnp.sum(ct[...], axis=0)
    nslot = 2 * NY
    npick = NZ * nslot
    ntok = NY * S
    ii = lax.broadcasted_iota(jnp.int32, (npick, ntok), 0)
    tt = lax.broadcasted_iota(jnp.int32, (npick, ntok), 1)
    target = (2 * ((ii // nslot) * NQ + q) + lax.rem(ii // NY, 2) + 1).astype(F32)
    same = lax.rem(ii, NY) == tt // S
    hits = [(mine[k : k + 1] == target) & same for k in range(2)]
    pk[...] = jnp.where(hits[0] | hits[1], 1.0, 0.0).astype(BF16)
    wt = jnp.where(hits[0], mine[2:3], 0.0) + jnp.where(hits[1], mine[3:4], 0.0)
    wt = wt.T
    whi = wt.astype(BF16)
    wmat[:, 0:npick] = whi
    wmat[:, npick : 2 * npick] = (wt - whi.astype(F32)).astype(BF16)

    resid_ref, gain_ref, mix_ref = get("resid"), get("gain"), get("mix")
    def row_of(ref, j):
        n = DX // 128
        return jnp.concatenate(
            [ref[j * n + i : j * n + i + 1, :].astype(F32) for i in range(n)], axis=1
        )

    for d in order(NX):
        x_cp[d].wait_recv()
    sumsq = jnp.zeros((S, 1), F32)
    gsum = jnp.zeros((S, 1), F32)
    for j in range(NX):
        proj = xbuf[0, j].astype(F32)
        for i in range(1, NX):
            proj = proj + xbuf[i, j].astype(F32)
        state = resid_ref[:, j * DX : (j + 1) * DX].astype(F32) + proj.astype(BF16).astype(F32)
        sumsq = sumsq + jnp.sum(state * state, axis=1, keepdims=True)
        scaled = state * row_of(gain_ref, j)
        gsum = gsum + jnp.sum(scaled * row_of(mix_ref, j), axis=1, keepdims=True)
        st[0, j] = state
        st[1, j] = scaled
    inverse = lax.rsqrt(sumsq / (NX * DX) + EPSILON)
    gate = 1.0 / (1.0 + jnp.exp(-(inverse * gsum)))
    ghi = gate.astype(BF16).astype(F32)
    lane = lax.broadcasted_iota(jnp.int32, (S, 128), 1)
    rows[y] = (st[1, t] * inverse).astype(BF16)
    gts[y] = jnp.where(lane == 0, ghi, jnp.where(lane == 1, gate - ghi, 0.0)).astype(BF16)

    y_cp, t_cp = {}, {}
    for d in order(NY):
        y_cp[d] = remote(rows.at[y], rows.at[y], yq, (d,), dev(z, ys[d], c, t))
    for d in order(NY):
        t_cp[d] = remote(gts.at[y], gts.at[y], tq, (d,), dev(z, ys[d], c, t))
    for d in order(NY):
        y_cp[d].wait_recv()

    own_rows = rows[...].reshape(ntok, DX)
    disp[...] = dot(pk[...], own_rows).astype(BF16).reshape(NZ, nslot, DX)
    er[c, z] = disp[z]
    z_cp, g_cp = {}, {}
    for d in order(NZ):
        z_cp[d] = remote(disp.at[zs[d]], er.at[c, z], zq, (d,), dev(zs[d], y, c, t))
    g_cp[0] = remote(disp.at[z], er.at[c, z], gq, (0,), partner)

    for d in order(NZ):
        w_cp[d].wait_recv()
    v_cp = remote(dw.at[c], dw.at[c], vq, (0,), partner)
    v_cp.wait_recv()

    nden = NC * NZ * FD
    dgw, duw, ddw = [
        dw[:, :, i].astype(F32).reshape(nden, DX).astype(BF16) for i in range(3)
    ]
    dchunk = ntok // NX
    psd[:, :, 0:nden] = dot_t(own_rows, dgw).astype(BF16).reshape(NX, dchunk, nden)
    psd[:, :, nden : 2 * nden] = dot_t(own_rows, duw).astype(BF16).reshape(NX, dchunk, nden)
    a_cp, e_cp = {}, {}
    for d in order(NX)[::-1]:
        a_cp[d] = remote(psd.at[xs[d]], prd.at[d - 1], aq, (d,), dev(z, y, c, xs[d]))
    nall = NC * npick
    chunk = nall // NX
    p_cp, h_cp = {}, {}

    def scatter(j):
        for d in order(NX)[::-1]:
            p_cp[j, d] = remote(
                psend.at[j, xs[d]],
                prec.at[j, d - 1],
                pq,
                (j, d - 1),
                dev(z, y, c, xs[d]),
            )

    def hidden(j):
        acc = psend[j, t].astype(F32)
        for d in order(NX):
            p_cp[j, d].wait_recv()
        for d in range(1, NX):
            acc = acc + prec[j, d - 1].astype(F32)
        hid[j, t] = swish(acc, CW)
        for d in order(NX)[::-1]:
            h_cp[j, d] = remote(
                hid.at[j, t], hid.at[j, t], hq, (j, d - 1), dev(z, y, c, xs[d])
            )

    def swish(acc, n):
        g, u = acc[:, :n], acc[:, n:]
        return (g / (1.0 + jnp.exp(-g)) * u).astype(BF16)

    for d in order(NZ):
        z_cp[d].wait_recv()
        g_cp[d] = remote(er.at[c, zb[d]], er.at[c, zb[d]], gq, (d,), partner)
    acc = psd[t].astype(F32)
    for d in order(NX):
        a_cp[d].wait_recv()
        acc = acc + prd[d - 1].astype(F32)
    hdd[t] = swish(acc, nden)
    for d in order(NX)[::-1]:
        e_cp[d] = remote(hdd.at[t], hdd.at[t], eq, (d,), dev(z, y, c, xs[d]))
    wg_v, wu_v = get("wg"), get("wu")
    for d in range(NZ):
        g_cp[d].wait_recv()
    picked = er[...].reshape(nall, DX)
    for j in range(NCH):
        psend[j, :, :, 0:CW] = (
            dot(picked, wg_v[:, j * CW : (j + 1) * CW]).astype(BF16).reshape(NX, chunk, CW)
        )
        psend[j, :, :, CW : 2 * CW] = (
            dot(picked, wu_v[:, j * CW : (j + 1) * CW]).astype(BF16).reshape(NX, chunk, CW)
        )
        scatter(j)
    for d in order(NY):
        t_cp[d].wait_recv()
    for d in order(NX):
        e_cp[d].wait_recv()
    gates = gts[...].reshape(ntok, 128)
    gates = gates[:, 0:1].astype(F32) + gates[:, 1:2].astype(F32)
    dacc[...] = gates * dot(hdd[...].reshape(ntok, nden), ddw)
    for j in range(NCH):
        hidden(j)
    wd_v = get("wd")
    half = NX // NC

    def down(which, j):
        rows_in = hid[j, pl.ds(which * half, half)].reshape(npick, CW)
        return dot(rows_in, wd_v[j * CW : (j + 1) * CW, :])

    for j in range(NCH):
        for d in order(NX):
            h_cp[j, d].wait_recv()
        if j == 0:
            theirs, ours = down(o, 0), down(c, 0)
        elif j < NCH - 1:
            theirs, ours = theirs + down(o, j), ours + down(c, j)
    if NCH > 1:
        theirs = theirs + down(o, NCH - 1)

    osend[...] = theirs.astype(BF16).reshape(NZ, nslot, DX)
    s_cp = remote(osend, orecv, sq, (0,), partner)
    if NCH > 1:
        ours = ours + down(c, NCH - 1)
    s_cp.wait_recv()
    ret[...] = (ours + orecv[...].reshape(npick, DX).astype(F32)).astype(BF16).reshape(
        NZ, nslot, DX
    )

    o_cp = {}
    for d in order(NZ)[::-1]:
        o_cp[d] = remote(ret.at[zs[d]], rb.at[z], oq, (d,), dev(zs[d], y, c, t))
    rb[z] = ret[z]
    for d in order(NZ):
        o_cp[d].wait_recv()
    back = rb[...].reshape(npick, DX)
    both = jnp.concatenate([back, back], axis=0)
    comb = dot(wmat[...], both) + dacc[...]
    csend[...] = comb.astype(BF16).reshape(NY, S, DX)

    b_cp = {}
    for d in order(NY)[::-1]:
        b_cp[d] = remote(csend.at[ys[d]], cb.at[y], bq, (d,), dev(z, ys[d], c, t))
    cb[y] = csend[y]
    for d in order(NY):
        b_cp[d].wait_recv()
    res = st[0, t]
    for yy in range(NY):
        res = res + cb[yy].astype(F32)
    out_ref[...] = res.astype(BF16)
    for d in sent:
        d.wait_send()


def body(
    resid,
    queries,
    new_keys,
    new_values,
    key_cache,
    value_cache,
    cum_gate,
    forget_logit,
    forget_bias,
    lengths,
    out_weight,
    norm_gain,
    mix_vector,
    routes,
    route_weight,
    expert_gate,
    expert_up,
    expert_down,
    dense_gate,
    dense_up,
    dense_down,
):
    NX = lax.axis_size("tp")
    n_ep = lax.axis_size("ep")
    NZ = n_ep // (NC * NY)
    S, D = resid.shape
    SLOTS = key_cache.shape[2]
    DX = D // NX
    FF = expert_gate.shape[2]
    FD = dense_gate.shape[1]
    CW = min(256, FF)
    NCH = FF // CW
    dims = (NX, NZ, S, SLOTS, DX, CW, NCH, FD)
    nslot = 2 * NY
    npick = NZ * nslot
    ntok = NY * S
    nden = NC * NZ * FD
    chunk = NC * npick // NX
    dchunk = ntok // NX
    vm = pl.BlockSpec(memory_space=pltpu.VMEM)
    hb = pl.BlockSpec(memory_space=pl.ANY)
    args = (
        resid,
        queries,
        new_keys,
        new_values,
        cum_gate,
        forget_logit.T,
        forget_bias.reshape(1, 2),
        lengths.reshape(1, S),
        routes.T,
        route_weight.T,
        norm_gain.reshape(D // 128, 128),
        mix_vector.reshape(D // 128, 128),
        key_cache.reshape(S * SLOTS, HEAD),
        value_cache.reshape(S * SLOTS, HEAD),
        out_weight,
        expert_gate[0],
        expert_up[0],
        expert_down[0],
        dense_gate.T,
        dense_up.T,
        dense_down,
    )
    scratch = [pltpu.VMEM(a.shape, a.dtype) for a in args[:18]]
    scratch += [
        pltpu.VMEM(*sd)
        for sd in (
            ((8, ntok), F32),
            ((NY, 8, ntok), F32),
            ((NC, NZ, 3, FD, DX), BF16),
            ((NX, NX, S, DX), BF16),
            ((2, NX, S, DX), F32),
            ((NY, S, DX), BF16),
            ((NY, S, 128), BF16),
            ((npick, ntok), BF16),
            ((ntok, 2 * npick), BF16),
            ((NZ, nslot, DX), BF16),
            ((NC, NZ, nslot, DX), BF16),
            ((NCH, NX, chunk, 2 * CW), BF16),
            ((NCH, NX - 1, chunk, 2 * CW), BF16),
            ((NCH, NX, chunk, CW), BF16),
            ((NX, dchunk, 2 * nden), BF16),
            ((NX - 1, dchunk, 2 * nden), BF16),
            ((NX, dchunk, nden), BF16),
            ((ntok, DX), F32),
            ((NZ, nslot, DX), BF16),
            ((NZ, nslot, DX), BF16),
            ((NZ, nslot, DX), BF16),
            ((NZ, nslot, DX), BF16),
            ((NY, S, DX), BF16),
            ((NY, S, DX), BF16),
        )
    ]
    dma = pltpu.SemaphoreType.DMA
    scratch += [dma((len(args),))]
    scratch += [
        dma((2, *n))
        for n in (
            (NX,),
            (NY,),
            (NZ,),
            (1,),
            (NY,),
            (NY,),
            (NZ,),
            (NZ,),
            (NCH, NX - 1),
            (NCH, NX - 1),
            (NX,),
            (NX,),
            (1,),
            (NZ,),
            (NY,),
        )
    ]
    return pl.pallas_call(
        functools.partial(kernel, dims),
        name="layer",
        out_shape=pltpu.VMEM((S, DX), BF16),
        in_specs=[hb] * len(args),
        out_specs=vm,
        scratch_shapes=scratch,
        compiler_params=pltpu.CompilerParams(
            collective_id=0, has_side_effects=True, vmem_limit_bytes=56 * 1024 * 1024
        ),
    )(*args)


def solution(mesh):
    return jax.shard_map(
        body,
        mesh=mesh,
        in_specs=(
            P("ep", None),
            P("ep", "tp"),
            P("ep", "tp"),
            P("ep", "tp"),
            P("ep", "tp", None, None),
            P("ep", "tp", None, None),
            P("ep", "tp", None),
            P("ep", "tp"),
            P("tp"),
            P("ep"),
            P("tp", None),
            P(),
            P(),
            P("ep", None),
            P("ep", None),
            P("ep", "tp", None),
            P("ep", "tp", None),
            P("ep", None, "tp"),
            P("tp", "ep"),
            P("tp", "ep"),
            P("ep", "tp"),
        ),
        out_specs=P("ep", "tp"),
        check_vma=False,
    )
```

time: 80.6 us -> 68 us (0.84)
  local copies, waits for them, and re-layouts: 7.72 us -> 0.61 us
  Pallas kernels: 70.4 us -> 67.3 us
  other arithmetic: 1.91 us -> 0 us
    unnamed x23 -> x1, local copies, waits for them, and re-layouts: 6.79 us -> 0.61 us
    pallas_call x1, Pallas kernels: 70.4 us -> 67.3 us  [body(): pl.pallas_call(functools.partial(kernel, dims), name='layer', out_shape=p...]
where the time goes in v2:
time: 68 us; the launch traced here: 67.9 us
  Pallas kernels  67.3 us (99%)
    pallas_call x1, Pallas kernels, body(): pl.pallas_call(functools.partial(kernel, dims), name='layer', out_shape=p...  67.3 us

profile of v2, /device:TPU:1, one launch (start us, length us, event | category | flops | bytes accessed | tf_op | source)
XLA Modules:
  0.0 67.9 jit_solution(4638319030665687678)
XLA Ops:
  0.0 67.3 %layer.1 = bf16[16,512]{1,0:T(8,128)(2,1)S(1)} custom-call(bf16[16,2048]{1,0:T(8,128)(2,1)} %refs_0_.1, bf16[16,256]{1,0:T(8,128)(2,1)} %refs_1_.1, bf16[16,128]{1,0:T(8,128)(2,1)} %refs_2_.1, bf16[16,128]{1,0:T(8,128)(2,1)} %refs_3_.1, f32[16,2,256]{2,1,0:T(2,128)} %refs_4_.1, f32[2,16]{1,0:T(2,128)} %bitcast.23, f32[1,2]{1,0:T(1,128)} %bitcast.26, ...), custom_call_target="tpu_custom_call" | custom-call | tf_op jit(solution)/shard_map/layer/pallas_call | solution.py:482
  67.3 0.6 copy.23

commit v3 on v2

--- a/solution.py
+++ b/solution.py
@@ -75,6 +75,14 @@
     def order(n):
         return sorted(range(1, n), key=lambda d: (min(d, n - d), d))
 
+    loads = {}
+    targets = dict(local, dg=dw.at[c, z, 0], du=dw.at[c, z, 1], dd=dw.at[c, z, 2])
+    first = ["q", "k", "len", "cg", "fl", "fb", "nk", "nv", "dg", "du", "dd", "v", "wo"]
+    first += ["rt", "rw", "resid", "gain", "mix"]
+    for i, name in enumerate(first + [a for a in ARGS if a not in first]):
+        loads[name] = pltpu.make_async_copy(h[name], targets[name], lsem.at[i])
+        loads[name].start()
+
     partner = dev(z, y, o, t)
     barrier = pltpu.get_barrier_semaphore()
     peers = [dev(z, y, c, xs[d]) for d in range(1, NX)]
@@ -84,14 +92,6 @@
     for p in peers:
         pl.semaphore_signal(barrier, inc=1, device_id=p, device_id_type=pl.DeviceIdType.MESH)
 
-    loads = {}
-    targets = dict(local, dg=dw.at[c, z, 0], du=dw.at[c, z, 1], dd=dw.at[c, z, 2])
-    first = ["q", "k", "len", "rt", "cg", "fl", "fb", "rw", "nk", "nv", "v", "wo"]
-    first += ["resid", "gain", "mix"]
-    for i, name in enumerate(first + [a for a in ARGS if a not in first]):
-        loads[name] = pltpu.make_async_copy(h[name], targets[name], lsem.at[i])
-        loads[name].start()
-
     def get(name):
         loads[name].wait()
         return local[name]
@@ -101,24 +101,6 @@
 
     def column(row):
         return jnp.sum(jnp.where(tr == tc, row, jnp.zeros_like(row)), axis=1, keepdims=True)
-
-    rt = get("rt")[...].astype(F32)
-    rw = get("rw")[...]
-    lanes = lax.broadcasted_iota(jnp.int32, (S, NY * S), 1)
-    place = lanes == y * S + lax.broadcasted_iota(jnp.int32, (S, NY * S), 0)
-    for k in range(2):
-        mine = column(rt[k : k + 1])
-        rank = jnp.zeros((S, 1), F32)
-        for i in range(2):
-            taken = (rt[i : i + 1] == mine) & (tc < tr)
-            rank = rank + jnp.sum(jnp.where(taken, 1.0, 0.0), axis=1, keepdims=True)
-        code = 2.0 * mine + rank + 1.0
-        codes[k : k + 1] = jnp.sum(jnp.where(place, code, 0.0), axis=0, keepdims=True)
-        codes[2 + k : 3 + k] = jnp.sum(
-            jnp.where(place, column(rw[k : k + 1]), 0.0), axis=0, keepdims=True
-        )
-    codes[4:8] = jnp.zeros((4, NY * S), F32)
-    ct[y] = codes[...]
 
     lens = column(get("len")[...])
     cg_ref, fl_ref, fb_ref = get("cg"), get("fl"), get("fb")
@@ -151,6 +133,21 @@
     total = jnp.sum(past, axis=1, keepdims=True) + wown
     probs = (past / total).astype(BF16).astype(F32)
     pown = (wown / total).astype(BF16).astype(F32)
+    pl.semaphore_wait(barrier, len(peers))
+    for name in ("dg", "du", "dd"):
+        loads[name].wait()
+    near = [d for d in order(NZ) if min(d, NZ - d) <= 2]
+    w_cp, v_cp = {}, {}
+    for d in near:
+        w_cp[d] = remote(dw.at[c, z], dw.at[c, z], wq, (d,), dev(zs[d], y, c, t))
+    v_cp[0] = remote(dw.at[c, z], dw.at[c, z], vq, (0,), partner)
+
+    def pass_on(d):
+        w_cp[d].wait_recv()
+        if d == NZ // 2 and NZ == 8:
+            w_cp[4, 1].wait_recv()
+        v_cp[d] = remote(dw.at[c, zb[d]], dw.at[c, zb[d]], vq, (d,), partner)
+
     v_v = get("v")
     mixed = pown * jnp.concatenate([nv, nv], axis=0)
     for s in range(S):
@@ -162,16 +159,30 @@
     wo_v = get("wo")
     for j in range(NX):
         xbuf[t, j] = dot(attended, wo_v[:, j * DX : (j + 1) * DX]).astype(BF16)
-    pl.semaphore_wait(barrier, len(peers))
-    x_cp, c_cp, w_cp = {}, {}, {}
+    x_cp, c_cp = {}, {}
     for d in order(NX):
         x_cp[d] = remote(xbuf.at[t], xbuf.at[t], xq, (d,), dev(z, y, c, xs[d]))
+
+    rt = get("rt")[...].astype(F32)
+    rw = get("rw")[...]
+    lanes = lax.broadcasted_iota(jnp.int32, (S, NY * S), 1)
+    place = lanes == y * S + lax.broadcasted_iota(jnp.int32, (S, NY * S), 0)
+    for k in range(2):
+        mine = column(rt[k : k + 1])
+        rank = jnp.zeros((S, 1), F32)
+        for i in range(2):
+            taken = (rt[i : i + 1] == mine) & (tc < tr)
+            rank = rank + jnp.sum(jnp.where(taken, 1.0, 0.0), axis=1, keepdims=True)
+        code = 2.0 * mine + rank + 1.0
+        codes[k : k + 1] = jnp.sum(jnp.where(place, code, 0.0), axis=0, keepdims=True)
+        codes[2 + k : 3 + k] = jnp.sum(
+            jnp.where(place, column(rw[k : k + 1]), 0.0), axis=0, keepdims=True
+        )
+    codes[4:8] = jnp.zeros((4, NY * S), F32)
+    ct[y] = codes[...]
+
     for d in order(NY):
         c_cp[d] = remote(codes, ct.at[y], cq, (d,), dev(z, ys[d], c, t))
-    for name in ("dg", "du", "dd"):
-        loads[name].wait()
-    for d in order(NZ):
-        w_cp[d] = remote(dw.at[c, z], dw.at[c, z], wq, (d,), dev(zs[d], y, c, t))
 
     for d in order(NY):
         c_cp[d].wait_recv()
@@ -224,6 +235,20 @@
         y_cp[d] = remote(rows.at[y], rows.at[y], yq, (d,), dev(z, ys[d], c, t))
     for d in order(NY):
         t_cp[d] = remote(gts.at[y], gts.at[y], tq, (d,), dev(z, ys[d], c, t))
+
+    for d in near:
+        pass_on(d)
+    if NZ == 8:
+        for d, to in ((2, 1), (6, 7)):
+            f = (to + d) % NZ
+            w_cp[f] = remote(
+                dw.at[c, zb[d]], dw.at[c, zb[d]], wq, (f,), dev(zs[to], y, c, t)
+            )
+        for i, d in enumerate((2, 6)):
+            part = (c, zb[d], slice(None), slice(None), pl.ds(i * (DX // 2), DX // 2))
+            f = remote(dw.at[part], dw.at[part], wq, (4 * (1 - i),), dev(zs[d], y, c, t))
+            w_cp[(4, 1) if i else 4] = f
+    far = [d for d in order(NZ) if d not in near]
     for d in order(NY):
         y_cp[d].wait_recv()
 
@@ -235,10 +260,11 @@
         z_cp[d] = remote(disp.at[zs[d]], er.at[c, z], zq, (d,), dev(zs[d], y, c, t))
     g_cp[0] = remote(disp.at[z], er.at[c, z], gq, (0,), partner)
 
-    for d in order(NZ):
-        w_cp[d].wait_recv()
-    v_cp = remote(dw.at[c], dw.at[c], vq, (0,), partner)
-    v_cp.wait_recv()
+    for d in far:
+        pass_on(d)
+
+    for d in range(NZ):
+        v_cp[d].wait_recv()
 
     nden = NC * NZ * FD
     dgw, duw, ddw = [
@@ -283,6 +309,20 @@
     for d in order(NZ):
         z_cp[d].wait_recv()
         g_cp[d] = remote(er.at[c, zb[d]], er.at[c, zb[d]], gq, (d,), partner)
+    wg_v, wu_v = get("wg"), get("wu")
+    for d in range(NZ):
+        g_cp[d].wait_recv()
+    picked = er[...].reshape(nall, DX)
+    for j in range(NCH):
+        psend[j, :, :, 0:CW] = (
+            dot(picked, wg_v[:, j * CW : (j + 1) * CW]).astype(BF16).reshape(NX, chunk, CW)
+        )
+        psend[j, :, :, CW : 2 * CW] = (
+            dot(picked, wu_v[:, j * CW : (j + 1) * CW]).astype(BF16).reshape(NX, chunk, CW)
+        )
+        scatter(j)
+    for j in range(NCH):
+        hidden(j)
     acc = psd[t].astype(F32)
     for d in order(NX):
         a_cp[d].wait_recv()
@@ -290,27 +330,6 @@
     hdd[t] = swish(acc, nden)
     for d in order(NX)[::-1]:
         e_cp[d] = remote(hdd.at[t], hdd.at[t], eq, (d,), dev(z, y, c, xs[d]))
-    wg_v, wu_v = get("wg"), get("wu")
-    for d in range(NZ):
-        g_cp[d].wait_recv()
-    picked = er[...].reshape(nall, DX)
-    for j in range(NCH):
-        psend[j, :, :, 0:CW] = (
-            dot(picked, wg_v[:, j * CW : (j + 1) * CW]).astype(BF16).reshape(NX, chunk, CW)
-        )
-        psend[j, :, :, CW : 2 * CW] = (
-            dot(picked, wu_v[:, j * CW : (j + 1) * CW]).astype(BF16).reshape(NX, chunk, CW)
-        )
-        scatter(j)
-    for d in order(NY):
-        t_cp[d].wait_recv()
-    for d in order(NX):
-        e_cp[d].wait_recv()
-    gates = gts[...].reshape(ntok, 128)
-    gates = gates[:, 0:1].astype(F32) + gates[:, 1:2].astype(F32)
-    dacc[...] = gates * dot(hdd[...].reshape(ntok, nden), ddw)
-    for j in range(NCH):
-        hidden(j)
     wd_v = get("wd")
     half = NX // NC
 
@@ -341,6 +360,13 @@
     for d in order(NZ)[::-1]:
         o_cp[d] = remote(ret.at[zs[d]], rb.at[z], oq, (d,), dev(zs[d], y, c, t))
     rb[z] = ret[z]
+    for d in order(NY):
+        t_cp[d].wait_recv()
+    for d in order(NX):
+        e_cp[d].wait_recv()
+    gates = gts[...].reshape(ntok, 128)
+    gates = gates[:, 0:1].astype(F32) + gates[:, 1:2].astype(F32)
+    dacc[...] = gates * dot(hdd[...].reshape(ntok, nden), ddw)
     for d in order(NZ):
         o_cp[d].wait_recv()
     back = rb[...].reshape(npick, DX)
@@ -465,7 +491,7 @@
             (NX,),
             (NY,),
             (NZ,),
-            (1,),
+            (NZ,),
             (NY,),
             (NY,),
             (NZ,),

time: 68 us -> 63.2 us (0.929)
  Pallas kernels: 67.3 us -> 62.5 us
    pallas_call x1, Pallas kernels: 67.3 us -> 62.5 us  [body(): pl.pallas_call(functools.partial(kernel, dims), name='layer', out_shape=p...]
where the time goes in v3:
time: 63.2 us; the launch traced here: 63.1 us
  Pallas kernels  62.5 us (99%)
    pallas_call x1, Pallas kernels, body(): pl.pallas_call(functools.partial(kernel, dims), name='layer', out_shape=p...  62.5 us

profile of v3, /device:TPU:1, one launch (start us, length us, event | category | flops | bytes accessed | tf_op | source)
XLA Modules:
  0.0 63.1 jit_solution(17558286222578434414)
XLA Ops:
  0.0 62.5 %layer.1 = bf16[16,512]{1,0:T(8,128)(2,1)S(1)} custom-call(bf16[16,2048]{1,0:T(8,128)(2,1)} %refs_0_.1, bf16[16,256]{1,0:T(8,128)(2,1)} %refs_1_.1, bf16[16,128]{1,0:T(8,128)(2,1)} %refs_2_.1, bf16[16,128]{1,0:T(8,128)(2,1)} %refs_3_.1, f32[16,2,256]{2,1,0:T(2,128)} %refs_4_.1, f32[2,16]{1,0:T(2,128)} %bitcast.23, f32[1,2]{1,0:T(1,128)} %bitcast.26, ...), custom_call_target="tpu_custom_call" | custom-call | tf_op jit(solution)/shard_map/layer/pallas_call | solution.py:508
  62.5 0.6 copy.23

commit v4 on v3

--- a/solution.py
+++ b/solution.py
@@ -160,7 +160,7 @@
     for j in range(NX):
         xbuf[t, j] = dot(attended, wo_v[:, j * DX : (j + 1) * DX]).astype(BF16)
     x_cp, c_cp = {}, {}
-    for d in order(NX):
+    for d in order(NX)[::-1]:
         x_cp[d] = remote(xbuf.at[t], xbuf.at[t], xq, (d,), dev(z, y, c, xs[d]))
 
     rt = get("rt")[...].astype(F32)
@@ -231,10 +231,8 @@
     gts[y] = jnp.where(lane == 0, ghi, jnp.where(lane == 1, gate - ghi, 0.0)).astype(BF16)
 
     y_cp, t_cp = {}, {}
-    for d in order(NY):
+    for d in order(NY)[::-1]:
         y_cp[d] = remote(rows.at[y], rows.at[y], yq, (d,), dev(z, ys[d], c, t))
-    for d in order(NY):
-        t_cp[d] = remote(gts.at[y], gts.at[y], tq, (d,), dev(z, ys[d], c, t))
 
     for d in near:
         pass_on(d)
@@ -256,9 +254,43 @@
     disp[...] = dot(pk[...], own_rows).astype(BF16).reshape(NZ, nslot, DX)
     er[c, z] = disp[z]
     z_cp, g_cp = {}, {}
-    for d in order(NZ):
+    for d in order(NZ)[::-1]:
         z_cp[d] = remote(disp.at[zs[d]], er.at[c, z], zq, (d,), dev(zs[d], y, c, t))
+    for d in order(NY):
+        t_cp[d] = remote(gts.at[y], gts.at[y], tq, (d,), dev(z, ys[d], c, t))
     g_cp[0] = remote(disp.at[z], er.at[c, z], gq, (0,), partner)
+
+    part = npick // NX
+    p_cp, h_cp = {}, {}
+
+    def scatter(half, j):
+        rows_in = er[(c, o)[half]].reshape(npick, DX)
+        for i, w in enumerate((wg_v, wu_v)):
+            psend[half, j, :, :, i * CW : (i + 1) * CW] = (
+                dot(rows_in, w[:, j * CW : (j + 1) * CW]).astype(BF16).reshape(NX, part, CW)
+            )
+        for d in order(NX)[::-1]:
+            key = (half, j, d - 1)
+            p_cp[key] = remote(
+                psend.at[half, j, xs[d]], prec.at[key], pq, key, dev(z, y, c, xs[d])
+            )
+
+    def hidden(j):
+        for half in range(2):
+            acc = psend[half, j, t].astype(F32)
+            for d in order(NX):
+                p_cp[half, j, d - 1].wait_recv()
+            for d in range(1, NX):
+                acc = acc + prec[half, j, d - 1].astype(F32)
+            hid[j, t, half] = swish(acc, CW)
+        for d in order(NX)[::-1]:
+            h_cp[j, d] = remote(
+                hid.at[j, t], hid.at[j, t], hq, (j, d - 1), dev(z, y, c, xs[d])
+            )
+
+    def swish(acc, n):
+        g, u = acc[:, :n], acc[:, n:]
+        return (g / (1.0 + jnp.exp(-g)) * u).astype(BF16)
 
     for d in far:
         pass_on(d)
@@ -276,51 +308,17 @@
     a_cp, e_cp = {}, {}
     for d in order(NX)[::-1]:
         a_cp[d] = remote(psd.at[xs[d]], prd.at[d - 1], aq, (d,), dev(z, y, c, xs[d]))
-    nall = NC * npick
-    chunk = nall // NX
-    p_cp, h_cp = {}, {}
-
-    def scatter(j):
-        for d in order(NX)[::-1]:
-            p_cp[j, d] = remote(
-                psend.at[j, xs[d]],
-                prec.at[j, d - 1],
-                pq,
-                (j, d - 1),
-                dev(z, y, c, xs[d]),
-            )
-
-    def hidden(j):
-        acc = psend[j, t].astype(F32)
-        for d in order(NX):
-            p_cp[j, d].wait_recv()
-        for d in range(1, NX):
-            acc = acc + prec[j, d - 1].astype(F32)
-        hid[j, t] = swish(acc, CW)
-        for d in order(NX)[::-1]:
-            h_cp[j, d] = remote(
-                hid.at[j, t], hid.at[j, t], hq, (j, d - 1), dev(z, y, c, xs[d])
-            )
-
-    def swish(acc, n):
-        g, u = acc[:, :n], acc[:, n:]
-        return (g / (1.0 + jnp.exp(-g)) * u).astype(BF16)
-
     for d in order(NZ):
         z_cp[d].wait_recv()
         g_cp[d] = remote(er.at[c, zb[d]], er.at[c, zb[d]], gq, (d,), partner)
     wg_v, wu_v = get("wg"), get("wu")
+    for j in range(NCH):
+        scatter(0, j)
+
     for d in range(NZ):
         g_cp[d].wait_recv()
-    picked = er[...].reshape(nall, DX)
     for j in range(NCH):
-        psend[j, :, :, 0:CW] = (
-            dot(picked, wg_v[:, j * CW : (j + 1) * CW]).astype(BF16).reshape(NX, chunk, CW)
-        )
-        psend[j, :, :, CW : 2 * CW] = (
-            dot(picked, wu_v[:, j * CW : (j + 1) * CW]).astype(BF16).reshape(NX, chunk, CW)
-        )
-        scatter(j)
+        scatter(1, j)
     for j in range(NCH):
         hidden(j)
     acc = psd[t].astype(F32)
@@ -331,26 +329,25 @@
     for d in order(NX)[::-1]:
         e_cp[d] = remote(hdd.at[t], hdd.at[t], eq, (d,), dev(z, y, c, xs[d]))
     wd_v = get("wd")
-    half = NX // NC
 
     def down(which, j):
-        rows_in = hid[j, pl.ds(which * half, half)].reshape(npick, CW)
+        rows_in = hid[j, :, which].reshape(npick, CW)
         return dot(rows_in, wd_v[j * CW : (j + 1) * CW, :])
 
     for j in range(NCH):
         for d in order(NX):
             h_cp[j, d].wait_recv()
         if j == 0:
-            theirs, ours = down(o, 0), down(c, 0)
+            theirs, ours = down(1, 0), down(0, 0)
         elif j < NCH - 1:
-            theirs, ours = theirs + down(o, j), ours + down(c, j)
+            theirs, ours = theirs + down(1, j), ours + down(0, j)
     if NCH > 1:
-        theirs = theirs + down(o, NCH - 1)
+        theirs = theirs + down(1, NCH - 1)
 
     osend[...] = theirs.astype(BF16).reshape(NZ, nslot, DX)
     s_cp = remote(osend, orecv, sq, (0,), partner)
     if NCH > 1:
-        ours = ours + down(c, NCH - 1)
+        ours = ours + down(0, NCH - 1)
     s_cp.wait_recv()
     ret[...] = (ours + orecv[...].reshape(npick, DX).astype(F32)).astype(BF16).reshape(
         NZ, nslot, DX
@@ -426,7 +423,7 @@
     npick = NZ * nslot
     ntok = NY * S
     nden = NC * NZ * FD
-    chunk = NC * npick // NX
+    part = npick // NX
     dchunk = ntok // NX
     vm = pl.BlockSpec(memory_space=pltpu.VMEM)
     hb = pl.BlockSpec(memory_space=pl.ANY)
@@ -468,9 +465,9 @@
             ((ntok, 2 * npick), BF16),
             ((NZ, nslot, DX), BF16),
             ((NC, NZ, nslot, DX), BF16),
-            ((NCH, NX, chunk, 2 * CW), BF16),
-            ((NCH, NX - 1, chunk, 2 * CW), BF16),
-            ((NCH, NX, chunk, CW), BF16),
+            ((2, NCH, NX, part, 2 * CW), BF16),
+            ((2, NCH, NX - 1, part, 2 * CW), BF16),
+            ((NCH, NX, 2, part, CW), BF16),
             ((NX, dchunk, 2 * nden), BF16),
             ((NX - 1, dchunk, 2 * nden), BF16),
             ((NX, dchunk, nden), BF16),
@@ -496,7 +493,7 @@
             (NY,),
             (NZ,),
             (NZ,),
-            (NCH, NX - 1),
+            (2, NCH, NX - 1),
             (NCH, NX - 1),
             (NX,),
             (NX,),

time: 63.2 us -> 61.6 us (0.975)
  Pallas kernels: 62.5 us -> 60.8 us
    pallas_call x1, Pallas kernels: 62.5 us -> 60.8 us  [body(): pl.pallas_call(functools.partial(kernel, dims), name='layer', out_shape=p...]
where the time goes in v4:
time: 61.6 us; the launch traced here: 61.5 us
  Pallas kernels  60.8 us (99%)
    pallas_call x1, Pallas kernels, body(): pl.pallas_call(functools.partial(kernel, dims), name='layer', out_shape=p...  60.8 us

profile of v4, /device:TPU:1, one launch (start us, length us, event | category | flops | bytes accessed | tf_op | source)
XLA Modules:
  0.0 61.5 jit_solution(4928505747955053573)
XLA Ops:
  0.0 60.8 %layer.1 = bf16[16,512]{1,0:T(8,128)(2,1)S(1)} custom-call(bf16[16,2048]{1,0:T(8,128)(2,1)} %refs_0_.1, bf16[16,256]{1,0:T(8,128)(2,1)} %refs_1_.1, bf16[16,128]{1,0:T(8,128)(2,1)} %refs_2_.1, bf16[16,128]{1,0:T(8,128)(2,1)} %refs_3_.1, f32[16,2,256]{2,1,0:T(2,128)} %refs_4_.1, f32[2,16]{1,0:T(2,128)} %bitcast.23, f32[1,2]{1,0:T(1,128)} %bitcast.26, ...), custom_call_target="tpu_custom_call" | custom-call | tf_op jit(solution)/shard_map/layer/pallas_call | solution.py:505
  60.8 0.6 copy.23
